TPU v7x, 32 devices: a whole 2x2x4 slice. The times are simulated.
32 devices in a mesh: sp: 16 (over z, y, x), tp: 2 (over core).
Axes of the slice: x: 2, y: 2, z: 4, core: 2. Of those that a mesh axis runs over, the one named last changes fastest.
Arguments:
- cotangent: bfloat16 [6144, 2048], P('sp'), may hold values from -6 to 6
- routes: int32 [6144, 2], P('sp'), may hold values from 0 to 15, all different within a row; in each aligned block of 384 rows (0 to 383, 384 to 767, ...) at most 72 rows name the same one
- route_weight: float32 [6144, 2], P('sp'), may hold values from 0.1 to 0.9
- expert_rows: bfloat16 [16, 1152, 2048], P('sp'), may hold values from -6 to 6
- gate_w: bfloat16 [16, 2048, 1024], P('sp', None, 'tp'), may hold values from -0.125 to 0.125
- up_w: bfloat16 [16, 2048, 1024], P('sp', None, 'tp'), may hold values from -0.125 to 0.125
- down_w: bfloat16 [16, 1024, 2048], P('sp', 'tp'), may hold values from -0.1875 to 0.1875
- in_x: bfloat16 [6144, 1024], P('sp', 'tp'), may hold values from -6 to 6
- in_y: bfloat16 [6144, 1024], P('sp', 'tp'), may hold values from -6 to 6
- state: bfloat16 [6144, 1024], P('sp', 'tp'), may hold values from -6 to 6
- conv_taps: float32 [4, 1024], P(None, 'tp'), may hold values from -3 to 3
- gate_a: bfloat16 [8, 128, 128], P('tp'), may hold values from -0.5 to 0.5
- gate_x: bfloat16 [8, 128, 128], P('tp'), may hold values from -0.5 to 0.5
- decay_rate: float32 [1024], P('tp'), as said below
- out_weight: bfloat16 [2048, 1024], P(None, 'tp'), may hold values from -0.1875 to 0.1875
Outputs:
- grad_gate: bfloat16 [16, 2048, 1024], P('sp', None, 'tp')
- grad_up: bfloat16 [16, 2048, 1024], P('sp', None, 'tp')
- grad_down: bfloat16 [16, 1024, 2048], P('sp', 'tp')
- grad_proj: float32 [2048, 1024], P('sp', 'tp')
- grad_x: float32 [6144, 1024], P('sp', 'tp')
- grad_y: float32 [6144, 1024], P('sp', 'tp')
Inputs may be any that keep to these rules, and one draw needn't show every extreme that they name: `routes`: among the 768 pairs of one device's rows no expert appears more than 72 times, and some expert appears exactly 72 times; a row's two experts differ. `decay_rate`: positive.
All inputs are finite; a program needn't handle non-finite values.
Results may differ from a plain program's by a relative error of at most 0.0052.
The roundings to bfloat16 on the way count: a program that leaves them out, or rounds other values in their place, can miss the bound.
Values may be sent and summed in bfloat16 or wider, within the bound.
A program may use at most 128 MiB of HBM per device.

v0:
```python
import jax
import jax.numpy as jnp
from jax import lax
from jax.sharding import PartitionSpec as P

rate_scale = 8.0
floor_square = 0.01
inv_root_two = 0.7071067811865476
inv_root_tau = 0.3989422804014327


def shifted(value, axis, by):
    devices = lax.axis_size(axis)
    pairs = [(i, i + by) for i in range(devices) if 0 <= i + by < devices]
    return lax.ppermute(value, axis, pairs)


def carried_in(value, axis, join, neutral):
    count, mine = (lax.axis_size(axis), lax.axis_index(axis))
    pieces = jax.tree.map(lambda part: lax.all_gather(part, axis), value)
    pieces = jax.tree.map(lambda part: part[::-1], pieces)
    mine = count - 1 - mine
    so_far = jax.tree.map(
        lambda part, zero: jnp.full_like(part, 0) + jnp.asarray(zero, part.dtype), value, neutral
    )

    def turn(position, so_far):
        longer = join(so_far, jax.tree.map(lambda part: part[position], pieces))
        return jax.tree.map(lambda new, old: jnp.where(position < mine, new, old), longer, so_far)

    return lax.fori_loop(0, count - 1, turn, so_far)


def linear_combine(earlier, later):
    return (earlier[0] * later[0], later[0] * earlier[1] + later[1])


def compose_maps(earlier, later):
    return (later[0] * earlier[0], later[1] + later[0] * earlier[1])


def body(
    cotangent,
    routes,
    route_weight,
    expert_rows,
    gate_w,
    up_w,
    down_w,
    in_x,
    in_y,
    state,
    conv_taps,
    gate_a,
    gate_x,
    decay_rate,
    out_weight,
):
    tokens, model_width = cotangent.shape
    experts = lax.axis_size("sp")
    core_count = lax.axis_size("tp")
    core_index = lax.axis_index("tp")
    per_token = routes.shape[1]
    capacity = expert_rows.shape[1] // experts
    half_width = model_width // core_count
    pair_expert = routes.reshape(-1)
    onehot = (pair_expert[:, None] == jnp.arange(experts, dtype=jnp.int32)[None, :]).astype(
        jnp.int32
    )
    before = jnp.cumsum(onehot, axis=0) - onehot
    position = jnp.sum(before * onehot, axis=1)
    target = pair_expert * capacity + position
    token_ids = jnp.repeat(jnp.arange(tokens, dtype=jnp.int32), per_token)
    slot_token = jnp.zeros((experts * capacity,), jnp.int32).at[target].set(token_ids)
    slot_weight = (
        jnp.zeros((experts * capacity,), jnp.float32).at[target].set(route_weight.reshape(-1))
    )
    own_cols = lax.dynamic_slice_in_dim(cotangent, core_index * half_width, half_width, 1)
    outgoing = (own_cols[slot_token].astype(jnp.float32) * slot_weight[:, None]).astype(
        jnp.bfloat16
    )
    arrived = lax.all_to_all(
        outgoing.reshape(experts, capacity, half_width),
        "sp",
        split_axis=0,
        concat_axis=0,
        tiled=True,
    )
    upstream = lax.all_gather(arrived.reshape(-1, half_width), "tp", axis=1, tiled=True)
    saved_rows = expert_rows[0]
    weight_gate = gate_w[0]
    weight_up = up_w[0]
    weight_down = down_w[0]
    pre_gate = jnp.dot(saved_rows, weight_gate, preferred_element_type=jnp.float32)
    pre_up = jnp.dot(saved_rows, weight_up, preferred_element_type=jnp.float32)
    gate_sigmoid = jax.nn.sigmoid(pre_gate)
    silu_value = pre_gate * gate_sigmoid
    active = (silu_value * pre_up).astype(jnp.bfloat16)
    inner = (((1,), (1,)), ((), ()))
    outer = (((0,), (0,)), ((), ()))
    grad_active = lax.dot_general(upstream, weight_down, inner, preferred_element_type=jnp.float32)
    grad_down = lax.dot_general(active, upstream, outer, preferred_element_type=jnp.float32).astype(
        jnp.bfloat16
    )
    up_adjoint = (grad_active * silu_value).astype(jnp.bfloat16)
    gate_adjoint = (
        grad_active * pre_up * gate_sigmoid * (1.0 + pre_gate * (1.0 - gate_sigmoid))
    ).astype(jnp.bfloat16)
    grad_gate = lax.dot_general(
        saved_rows, gate_adjoint, outer, preferred_element_type=jnp.float32
    ).astype(jnp.bfloat16)
    grad_up = lax.dot_general(
        saved_rows, up_adjoint, outer, preferred_element_type=jnp.float32
    ).astype(jnp.bfloat16)
    partial_value = lax.dot_general(
        gate_adjoint, weight_gate, inner, preferred_element_type=jnp.float32
    )
    partial_value = (
        partial_value
        + lax.dot_general(up_adjoint, weight_up, inner, preferred_element_type=jnp.float32)
    ).astype(jnp.bfloat16)
    summed = lax.psum_scatter(partial_value, "tp", scatter_dimension=1, tiled=True).astype(
        jnp.float32
    )
    returning = summed.astype(jnp.bfloat16).reshape(experts, capacity, half_width)
    returned = lax.all_to_all(returning, "sp", split_axis=0, concat_axis=0, tiled=True)
    picked = (
        returned.reshape(experts * capacity, half_width)[target]
        .astype(jnp.float32)
        .reshape(tokens, per_token, half_width)
    )
    stream_half = (own_cols.astype(jnp.float32) + jnp.sum(picked, axis=1)).astype(jnp.bfloat16)
    stream = lax.all_gather(stream_half, "tp", axis=1, tiled=True)
    y_float = in_y.astype(jnp.float32)
    gelu_y = jax.nn.gelu(y_float, approximate=False)
    gelu_slope = (
        0.5 * (1.0 + lax.erf(y_float * inv_root_two))
        + y_float * jnp.exp(-0.5 * y_float * y_float) * inv_root_tau
    )
    state_float = state.astype(jnp.float32)
    mixed_out = (state_float * gelu_y).astype(jnp.bfloat16)
    grad_proj = lax.psum_scatter(
        lax.dot_general(stream, mixed_out, outer, preferred_element_type=jnp.float32),
        "sp",
        scatter_dimension=0,
        tiled=True,
    )
    grad_mixed = jnp.dot(stream, out_weight, preferred_element_type=jnp.float32)
    grad_y = grad_mixed * state_float * gelu_slope
    grad_state = grad_mixed * gelu_y
    tap_count = conv_taps.shape[0]
    channels = in_x.shape[1]
    edge_rows = jnp.concatenate([in_x[tokens - tap_count + 1 :], state[tokens - 1 :]], axis=0)
    prior_rows = shifted(edge_rows, "sp", 1)
    extended = jnp.concatenate([prior_rows[: tap_count - 1], in_x], axis=0).astype(jnp.float32)
    state_prev = jnp.concatenate([prior_rows[tap_count - 1 :], state[:-1]], axis=0).astype(
        jnp.float32
    )
    conv_x = conv_taps[0][None, :] * extended[0:tokens]
    for offset in range(1, tap_count):
        conv_x = conv_x + conv_taps[offset][None, :] * extended[offset : offset + tokens]
    blocks = gate_a.shape[0]
    block_span = gate_a.shape[1]
    conv_b = conv_x.astype(jnp.bfloat16).reshape(tokens, blocks, block_span)
    keep_gate = jax.nn.sigmoid(
        jnp.einsum("tci,cij->tcj", conv_b, gate_a, preferred_element_type=jnp.float32)
    ).reshape(tokens, channels)
    input_gate = jax.nn.sigmoid(
        jnp.einsum("tci,cij->tcj", conv_b, gate_x, preferred_element_type=jnp.float32)
    ).reshape(tokens, channels)
    decay_step = jnp.exp(-rate_scale * keep_gate * decay_rate[None, :])
    norm_factor = jnp.sqrt(1.0 - decay_step * decay_step + floor_square)
    ahead_decay = jnp.concatenate([decay_step[1:], jnp.ones((1, channels), jnp.float32)], axis=0)
    scanned = lax.associative_scan(linear_combine, (ahead_decay[::-1], grad_state[::-1]), axis=0)
    products = scanned[0][::-1]
    local_adjoint = scanned[1][::-1]
    total_decay = decay_step[0] * products[0]
    total_carry = decay_step[0] * local_adjoint[0]
    carry_in = carried_in(
        (total_decay, total_carry),
        "sp",
        compose_maps,
        (jnp.ones_like(total_decay), jnp.zeros_like(total_carry)),
    )
    adjoint = local_adjoint + products * carry_in[1][None, :]
    grad_norm = adjoint * conv_x * input_gate
    log_grad = adjoint * decay_step * state_prev - grad_norm * decay_step * decay_step / norm_factor
    keep_adjoint = (
        log_grad * (-rate_scale * decay_rate[None, :]) * keep_gate * (1.0 - keep_gate)
    ).astype(jnp.bfloat16)
    input_adjoint = (adjoint * conv_x * norm_factor * input_gate * (1.0 - input_gate)).astype(
        jnp.bfloat16
    )
    back_keep = jnp.einsum(
        "tcj,cij->tci",
        keep_adjoint.reshape(tokens, blocks, block_span),
        gate_a,
        preferred_element_type=jnp.float32,
    )
    back_input = jnp.einsum(
        "tcj,cij->tci",
        input_adjoint.reshape(tokens, blocks, block_span),
        gate_x,
        preferred_element_type=jnp.float32,
    )
    conv_grad = (
        adjoint * input_gate * norm_factor
        + back_keep.reshape(tokens, channels)
        + back_input.reshape(tokens, channels)
    )
    later_rows = shifted(conv_grad[: tap_count - 1], "sp", -1)
    padded_grad = jnp.concatenate([conv_grad, later_rows], axis=0)
    grad_x = conv_taps[0][None, :] * padded_grad[tap_count - 1 : tap_count - 1 + tokens]
    for offset in range(1, tap_count):
        grad_x = (
            grad_x
            + conv_taps[offset][None, :]
            * padded_grad[tap_count - 1 - offset : tap_count - 1 - offset + tokens]
        )
    return (grad_gate[None], grad_up[None], grad_down[None], grad_proj, grad_x, grad_y)


def solution(mesh):
    in_specs = (
        P("sp", None),
        P("sp", None),
        P("sp", None),
        P("sp", None, None),
        P("sp", None, "tp"),
        P("sp", None, "tp"),
        P("sp", "tp", None),
        P("sp", "tp"),
        P("sp", "tp"),
        P("sp", "tp"),
        P(None, "tp"),
        P("tp", None, None),
        P("tp", None, None),
        P("tp"),
        P(None, "tp"),
    )
    out_specs = (
        P("sp", None, "tp"),
        P("sp", None, "tp"),
        P("sp", "tp", None),
        P("sp", "tp"),
        P("sp", "tp"),
        P("sp", "tp"),
    )
    return jax.shard_map(body, mesh=mesh, in_specs=in_specs, out_specs=out_specs, check_vma=False)
```

profile of v0, /device:TPU:4, one launch (start us, length us, event | category | flops | bytes accessed | tf_op | source)
XLA Modules:
  0.0 474.0 jit_solution(16874782598220482494)
XLA Ops:
  20.9 5.0 %gather_fusion = bf16[1152,1024]{1,0:T(8,128)(2,1)} fusion(bf16[384,1024]{1,0:T(8,128)(2,1)S(1)} %constant_dynamic-slice_fusion.2, s32[2048]{0:T(1024)S(1)} %pad_clamp_fusion), kind=kCustom, calls=%fused_computation | custom fusion | bytes 4723200 | tf_op jit(solution)/shard_map/gather | solution.py:79
  27.9 61.0 %all_to_all.10 = bf16[16,72,1024]{2,1,0:T(8,128)(2,1)} all-to-all(bf16[16,72,1024]{2,1,0:T(8,128)(2,1)S(1)} %fusion), channel_id=1, replica_groups=mesh['sp'=16,'tp'=2] {'sp'}, dimensions={0} | all-to-all | bytes 4718592 | tf_op jit(solution)/shard_map/all_to_all | solution.py:82
  89.5 6.6 %fusion.5 = f32[1152,512]{1,0:T(8,128)} fusion(bf16[1,1152,2048]{2,1,0:T(8,128)(2,1)} %param.20, bf16[1,2048,512]{2,1,0:T(8,128)(2,1)S(1)} %copy-done), kind=kOutput, calls=%fused_computation.14 | convolution fusion | flops 2415919104 | bytes 9175040 | tf_op jit(solution)/shard_map/dot_general | solution.py:94
  96.1 7.0 %fusion.7 = f32[1152,512]{1,0:T(8,128)} fusion(bf16[1,1152,2048]{2,1,0:T(8,128)(2,1)} %param.20, bf16[1,2048,512]{2,1,0:T(8,128)(2,1)S(1)} %copy-done.66), kind=kOutput, calls=%fused_computation.16 | convolution fusion | flops 2415919104 | bytes 9175040 | tf_op jit(solution)/shard_map/dot_general | solution.py:95
  103.1 7.8 %multiply_convert_fusion.1 = (bf16[1152,512]{1,0:T(8,128)(2,1)S(1)}, bf16[1152,512]{1,0:T(8,128)(2,1)S(1)}) fusion(f32[1152,512]{1,0:T(8,128)} %fusion.5, f32[1152,512]{1,0:T(8,128)} %fusion.7, bf16[1152,2048]{1,0:T(8,128)(2,1)} %all-gather.5.cloned.1.call-done, bf16[1,512,2048]{2,1,0:T(8,128)(2,1)} %param.23), kind=kOutput, calls=%fused_computation.25 | convolution fusion | flops 2423586816 | bytes 13893632 | tf_op jit(solution)/shard_map/dot_general | solution.py:101
  113.5 4.3 add_convert_fusion
  117.9 13.0 %reduce-scatter.3.cloned.1.call-done = bf16[1152,1024]{1,0:T(8,128)(2,1)} async-done(((bf16[1152,2048]{1,0:T(8,128)(2,1)}), bf16[1152,1024]{1,0:T(8,128)(2,1)}) %reduce-scatter.3.cloned.1.call-update) | async-done | bytes 2359312 | tf_op jit(solution)/shard_map/reduce_scatter | solution.py:122
  131.0 7.1 %all-to-all-start.1 = ((bf16[16,72,1024]{2,1,0:T(8,128)(2,1)}), bf16[16,72,1024]{2,1,0:T(8,128)(2,1)S(1)}, u32[]{:S(2)}, u32[]{:S(2)}) async-start(bf16[16,72,1024]{2,1,0:T(8,128)(2,1)} %bitcast.138), calls=%async_computation.2 | async-start | bytes 4718592 | tf_op jit(solution)/shard_map/all_to_all | solution.py:126
  141.9 4.9 %collective-permute-done = bf16[4,512]{1,0:T(4,128)(2,1)S(1)} collective-permute-done((bf16[4,512]{1,0:T(4,128)(2,1)S(1)}, bf16[4,512]{1,0:T(4,128)(2,1)S(1)}, u32[]{:S(2)}, u32[]{:S(2)}) %collective-permute-start) | collective-permute-done | bytes 4128 | tf_op jit(solution)/shard_map/ppermute | solution.py:15
  151.9 35.6 %all-to-all-done.1 = bf16[16,72,1024]{2,1,0:T(8,128)(2,1)S(1)} async-done(((bf16[16,72,1024]{2,1,0:T(8,128)(2,1)}), bf16[16,72,1024]{2,1,0:T(8,128)(2,1)S(1)}, u32[]{:S(2)}, u32[]{:S(2)}) %all-to-all-start.1) | async-done | bytes 2359328 | tf_op jit(solution)/shard_map/all_to_all | solution.py:126
  191.0 4.8 %reshape.126 = f32[384,2,1024]{2,1,0:T(2,128)} reshape(bf16[768,1024]{1,0:T(8,128)(2,1)} %gather_fusion.1) | data formatting | bytes 4718592 | tf_op jit(solution)/shard_map/convert_element_type | solution.py:129
  195.8 5.6 %reduce_sum.22 = f32[384,1024]{1,0:T(8,128)S(1)} reduce(f32[384,2,1024]{2,1,0:T(2,128)} %reshape.126, f32[]{:T(128)} %constant.56.clone.1), dimensions={1}, to_apply=%region_6.7 | reduce | flops 393216 | bytes 4718596 | tf_op jit(solution)/shard_map/reduce_sum | solution.py:132
  213.1 7.1 %fusion.19 = bf16[1,2048,512]{1,2,0:T(8,128)(2,1)} fusion(bf16[1152,512]{1,0:T(8,128)(2,1)} %copy-done.70, bf16[1,1152,2048]{2,1,0:T(8,128)(2,1)} %param.20), kind=kOutput, calls=%fused_computation.23 | convolution fusion | flops 2416967680 | bytes 7995392 | tf_op jit(solution)/shard_map/dot_general | solution.py:109
  220.2 6.9 %fusion.15 = bf16[1,512,2048]{2,1,0:T(8,128)(2,1)} fusion(bf16[1152,2048]{1,0:T(8,128)(2,1)} %all-gather.5.cloned.1.call-done, f32[1152,512]{1,0:T(8,128)S(1)} %copy-done.72, f32[1152,512]{1,0:T(8,128)S(1)} %copy-done.71), kind=kOutput, calls=%fused_computation.21 | convolution fusion | flops 2420506624 | bytes 11534336 | tf_op jit(solution)/shard_map/dot_general | solution.py:102
  227.1 6.1 %fusion.129 = (f32[384,512]{1,0:T(8,128)S(1)}, f32[384,512]{1,0:T(8,128)}, f32[384,512]{1,0:T(8,128)}) fusion(bf16[384,512]{1,0:T(8,128)(2,1)} %param.25, bf16[384,512]{1,0:T(8,128)(2,1)S(1)} %copy-done.10, bf16[384,2048]{1,0:T(8,128)(2,1)} %all-gather.7.cloned.1.call-done, bf16[2048,512]{1,0:T(8,128)(2,1)} %param.31), kind=kOutput, calls=%fused_computation.219 | convolution fusion | flops 820445184 | bytes 6815744 | tf_op jit(solution)/shard_map/dot_general | solution.py:148
  235.2 4.5 slice.352
  309.8 4.5 fusion.93
  331.5 6.8 %rev.14 = f32[384,512]{1,0:T(8,128)} reverse(f32[384,512]{1,0:T(8,128)} %add.324), dimensions={0} | reverse | bytes 1572864 | tf_op jit(solution)/shard_map/rev | solution.py:176
  347.4 6.9 %rev.15 = f32[384,512]{1,0:T(8,128)} reverse(f32[384,512]{1,0:T(8,128)} %add.332), dimensions={0} | reverse | bytes 1572864 | tf_op jit(solution)/shard_map/rev | solution.py:175
  355.1 40.4 %all-gather = f32[16,1,512]{2,1,0:T(1,128)S(1)} all-gather(f32[1,1,512]{2,1,0:T(1,128)S(1)} %get-tuple-element.163), channel_id=1, replica_groups=mesh['sp'=16,'tp'=2] {'sp'}, dimensions={0}, use_global_device_ids=true | all-gather | bytes 34816 | tf_op jit(solution)/shard_map/all_gather | solution.py:20
  395.6 35.5 %all-gather.1 = f32[16,1,512]{2,1,0:T(1,128)S(1)} all-gather(f32[1,1,512]{2,1,0:T(1,128)S(1)} %get-tuple-element.162), channel_id=1, replica_groups=mesh['sp'=16,'tp'=2] {'sp'}, dimensions={0}, use_global_device_ids=true | all-gather | bytes 34816 | tf_op jit(solution)/shard_map/all_gather | solution.py:20
  444.1 7.3 %collective-permute-start.1 = (f32[3,512]{1,0:T(4,128)S(1)}, f32[3,512]{1,0:T(4,128)S(1)}, u32[]{:S(2)}, u32[]{:S(2)}) collective-permute-start(f32[3,512]{1,0:T(4,128)S(1)} %slice.498), channel_id=1, source_target_pairs={{2,0},{4,2},{6,4},{8,6},{10,8},{12,10},{14,12},{16,14},{18,16},{20... | collective-permute-start | bytes 18440 | tf_op jit(solution)/shard_map/ppermute | solution.py:15
  451.4 6.4 %fusion.16 = bf16[1,2048,512]{1,2,0:T(8,128)(2,1)} fusion(bf16[1152,512]{1,0:T(8,128)(2,1)S(1)} %copy-done.69, bf16[1,1152,2048]{2,1,0:T(8,128)(2,1)} %param.20), kind=kOutput, calls=%fused_computation.22 | convolution fusion | flops 2416967680 | bytes 7995392 | tf_op jit(solution)/shard_map/dot_general | solution.py:112
  457.9 4.1 copy.65
  (382 shorter events, 159.7 us)
Async XLA Ops:
  7.2 82.3 %copy-start = (bf16[1,2048,512]{2,1,0:T(8,128)(2,1)S(1)}, bf16[1,2048,512]{2,1,0:T(8,128)(2,1)}, u32[]{:S(2)}) copy-start(bf16[1,2048,512]{2,1,0:T(8,128)(2,1)} %param.21) | copy-start | bytes 6291460
  7.2 95.9 %all-gather.5.cloned.1.call-start = ((), (), s32[]{:S(2)}) async-start(), calls=%async_computation.4 | async-start | bytes 7077888 | tf_op jit(solution)/shard_map/all_gather | solution.py:89
  88.9 42.0 %reduce-scatter.3.cloned.1.call-start = ((), (), s32[]{:S(2)}) async-start(), calls=%async_computation.5 | async-start | bytes 7077888 | tf_op jit(solution)/shard_map/reduce_scatter | solution.py:122
  131.0 7.2 %copy-start.10 = (bf16[384,512]{1,0:T(8,128)(2,1)S(1)}, bf16[384,512]{1,0:T(8,128)(2,1)}, u32[]{:S(2)}) copy-start(bf16[384,512]{1,0:T(8,128)(2,1)} %param.26) | copy-start | bytes 1179652
  131.0 7.2 %copy-start.20 = (bf16[384,512]{1,0:T(8,128)(2,1)S(1)}, bf16[384,512]{1,0:T(8,128)(2,1)}, u32[]{:S(2)}) copy-start(bf16[384,512]{1,0:T(8,128)(2,1)} %param.24) | copy-start | bytes 1179652
  131.0 10.8 %copy-start.65 = (f32[512]{0:T(512)S(1)}, f32[512]{0:T(512)}, u32[]{:S(2)}) copy-start(f32[512]{0:T(512)} %param.30) | copy-start | bytes 6148
  131.0 10.8 %copy-start.64 = (f32[4,512]{1,0:T(4,128)S(1)}, f32[4,512]{1,0:T(4,128)}, u32[]{:S(2)}) copy-start(f32[4,512]{1,0:T(4,128)} %param.27) | copy-start | bytes 24580
  131.0 56.5 %all-to-all-start.1 = ((bf16[16,72,1024]{2,1,0:T(8,128)(2,1)}), bf16[16,72,1024]{2,1,0:T(8,128)(2,1)S(1)}, u32[]{:S(2)}, u32[]{:S(2)}) async-start(bf16[16,72,1024]{2,1,0:T(8,128)(2,1)} %bitcast.138), calls=%async_computation.2 | async-start | bytes 4718592 | tf_op jit(solution)/shard_map/all_to_all | solution.py:126
  138.1 89.0 %all-gather.7.cloned.1.call-start = ((), (), s32[]{:S(2)}) async-start(), calls=%async_computation.6 | async-start | bytes 2359296 | tf_op jit(solution)/shard_map/all_gather | solution.py:133
  138.2 8.6 %collective-permute-start = (bf16[4,512]{1,0:T(4,128)(2,1)S(1)}, bf16[4,512]{1,0:T(4,128)(2,1)S(1)}, u32[]{:S(2)}, u32[]{:S(2)}) collective-permute-start(bf16[4,512]{1,0:T(4,128)(2,1)S(1)} %pad_maximum_fusion.14), channel_id=1, source_target_pairs={{0,2},{2,4},{4,6},{6,8},{8,10},{10,12},{12,14},{14,16},{16,18},{18... | collective-permute-start | bytes 12296 | tf_op jit(solution)/shard_map/ppermute | solution.py:15
  141.8 9.1 %copy-start.34 = (f32[512]{0:T(512)}, f32[512]{0:T(512)S(1)}, u32[]{:S(2)}) copy-start(f32[512]{0:T(512)S(1)} %broadcast_multiply_fusion.1) | copy-start | bytes 6148
  203.8 263.4 %reduce-scatter.5.cloned.1.call-start = ((), (), s32[]{:S(2)}) async-start(), calls=%async_computation.7 | async-start | bytes 4456448 | tf_op jit(solution)/shard_map/reduce_scatter | solution.py:142
  247.0 62.7 %copy-start.7 = (bf16[384,2048]{1,0:T(8,128)(2,1)S(1)}, bf16[384,2048]{1,0:T(8,128)(2,1)}, u32[]{:S(2)}) copy-start(bf16[384,2048]{1,0:T(8,128)(2,1)} %all-gather.7.cloned.1.call-done) | copy-start | bytes 4718596
  319.7 8.3 %copy-start.12 = (f32[191,512]{1,0:T(8,128)S(1)}, f32[191,512]{1,0:T(8,128)}, u32[]{:S(2)}) copy-start(f32[191,512]{1,0:T(8,128)} %slice.346) | copy-start | bytes 1173508
  329.1 9.2 %copy-start.14 = (f32[191,512]{1,0:T(8,128)S(1)}, f32[191,512]{1,0:T(8,128)}, u32[]{:S(2)}) copy-start(f32[191,512]{1,0:T(8,128)} %get-tuple-element.164) | copy-start | bytes 1173508
  330.3 11.6 %copy-start.6 = (f32[384,512]{1,0:T(8,128)}, f32[384,512]{1,0:T(8,128)S(1)}, u32[]{:S(2)}) copy-start(f32[384,512]{1,0:T(8,128)S(1)} %pad.115) | copy-start | bytes 2359300
  344.8 86.4 %copy-start.32 = (f32[512]{0:T(512)S(1)}, f32[512]{0:T(512)}, u32[]{:S(2)}) copy-start(f32[512]{0:T(512)} %custom-call) | copy-start | bytes 6148
  344.8 87.3 %copy-start.2 = (f32[384,512]{1,0:T(8,128)S(1)}, f32[384,512]{1,0:T(8,128)}, u32[]{:S(2)}) copy-start(f32[384,512]{1,0:T(8,128)} %get-tuple-element.156) | copy-start | bytes 2359300
  344.8 87.3 %copy-start.11 = (bf16[384,512]{1,0:T(8,128)(2,1)S(1)}, bf16[384,512]{1,0:T(8,128)(2,1)}, u32[]{:S(2)}) copy-start(bf16[384,512]{1,0:T(8,128)(2,1)} %param.26) | copy-start | bytes 1179652
  344.8 87.3 %copy-start.35 = (f32[512]{0:T(512)S(1)}, f32[512]{0:T(512)}, u32[]{:S(2)}) copy-start(f32[512]{0:T(512)} %copy-done.34) | copy-start | bytes 6148
  344.8 87.3 %copy-start.50 = (bf16[1,512]{1,0:T(2,128)(2,1)S(1)}, bf16[1,512]{1,0:T(2,128)(2,1)}, u32[]{:S(2)}) copy-start(bf16[1,512]{1,0:T(2,128)(2,1)} %slice.497) | copy-start | bytes 3076
  441.3 10.2 %copy-start.69 = (bf16[1152,512]{1,0:T(8,128)(2,1)S(1)}, bf16[1152,512]{1,0:T(8,128)(2,1)}, u32[]{:S(2)}) copy-start(bf16[1152,512]{1,0:T(8,128)(2,1)} %copy-done.68) | copy-start | bytes 3538948
  444.1 21.9 %collective-permute-start.1 = (f32[3,512]{1,0:T(4,128)S(1)}, f32[3,512]{1,0:T(4,128)S(1)}, u32[]{:S(2)}, u32[]{:S(2)}) collective-permute-start(f32[3,512]{1,0:T(4,128)S(1)} %slice.498), channel_id=1, source_target_pairs={{2,0},{4,2},{6,4},{8,6},{10,8},{12,10},{14,12},{16,14},{18,16},{20... | collective-permute-start | bytes 18440 | tf_op jit(solution)/shard_map/ppermute | solution.py:15
  457.9 9.4 %copy-start.1 = (bf16[1,2048,512]{2,1,0:T(8,128)(2,1)S(1)}, bf16[1,2048,512]{2,1,0:T(8,128)(2,1)}, u32[]{:S(2)}) copy-start(bf16[1,2048,512]{2,1,0:T(8,128)(2,1)} %param.21) | copy-start | bytes 6291460
  (56 other events, 146.7 us)
Sparse Core Ops, SparseCore 0:
  89.1 13.1 all-gather.4
  118.0 12.8 reduce-scatter.2
  203.9 18.8 all-gather.6
  314.6 102.3 reduce-scatter.4
where the time goes:
time: 483 us; the launch traced here: 474 us
  local copies, waits for them, and re-layouts  143 us (30%)
  blocking collectives  137 us (28%)
  matrix products  64.6 us (13%)
  waiting for transfers between devices  53.6 us (11%)
  other arithmetic  40.9 us (8%)
  starting transfers between devices  18.6 us (4%)
  between operations  15.5 us (3%)
    slice x61, local copies, waits for them, and re-layouts, body(): lax.associative_scan(linear_combine, (ahead_decay[::-1], grad_state[::-1]...  77.2 us
    all_gather x2, blocking collectives, carried_in(): pieces = jax.tree.map(lambda part: lax.all_gather(part, axis), value)  75.9 us
    all_to_all x1, blocking collectives, body(): lax.all_to_all(outgoing.reshape(experts, capacity, half_width), 'sp', spl...  61 us
    all_to_all x1, waiting for transfers between devices, body(): lax.all_to_all(returning, 'sp', split_axis=0, concat_axis=0, tiled=True)  35.6 us
    reduce_scatter x1, waiting for transfers between devices, body(): lax.psum_scatter(partial_value, 'tp', scatter_dimension=1, tiled=True)  13 us
    unnamed x152, local copies, waits for them, and re-layouts  11.6 us
    ppermute x2, starting transfers between devices, shifted(): return lax.ppermute(value, axis, pairs)  10.8 us
    pad x30, local copies, waits for them, and re-layouts, body(): lax.associative_scan(linear_combine, (ahead_decay[::-1], grad_state[::-1]...  10.4 us
  transfers between devices with their start and end apart: 7, of which 3 were waited for; matrix products, arithmetic and copies ran while one was open for 23% of the time, Pallas kernels for 0%

commit v1 on v0

v1 whole, which is shorter than its diff:
```python
import functools

import jax
import jax.numpy as jnp
from jax import lax
from jax.experimental import pallas as pl
from jax.experimental.pallas import tpu as pltpu
from jax.sharding import PartitionSpec as P


rate_scale = 8.0
floor_square = 0.01
inv_root_two = 0.7071067811865476
inv_root_tau = 0.3989422804014327
lanes_of_rows = 8
MESH = pl.DeviceIdType.MESH


def shifted(value, axis, by):
    devices = lax.axis_size(axis)
    pairs = [(i, i + by) for i in range(devices) if 0 <= i + by < devices]
    return lax.ppermute(value, axis, pairs)


def from_other_core(value):
    return lax.ppermute(value, "tp", [(0, 1), (1, 0)])


def both_halves(mine):
    other = from_other_core(mine)
    first = lax.axis_index("tp") == 0
    return jnp.concatenate(
        [jnp.where(first, mine, other), jnp.where(first, other, mine)], axis=1
    )


def recurrence_kernel(
    count,
    grad_state,
    decay_step,
    conv_x,
    keep_gate,
    input_gate,
    state_prev,
    gate_a,
    gate_x,
    decay_rate,
    conv_taps,
    grad_x,
    local_adjoint,
    products,
    conv_grad,
    totals,
    halo,
    send_sem,
    recv_sem,
    halo_send,
    halo_recv,
):
    tokens, channels = grad_state.shape
    segments = lanes_of_rows
    assert tokens % segments == 0
    span = tokens // segments
    me = lax.axis_index("sp")
    barrier = pltpu.get_barrier_semaphore()
    for step in range(1, count):
        pl.semaphore_signal(
            barrier, inc=1, device_id={"sp": lax.rem(me + step, count)}, device_id_type=MESH
        )

    pieces, _, piece_width = local_adjoint.shape
    for piece in range(pieces):
        cols = slice(piece * piece_width, (piece + 1) * piece_width)
        local_adjoint[piece] = grad_state[:, cols]
        products[piece] = decay_step[:, cols]

    def scan_step(step, carry):
        rows = pl.ds(span - 1 - step, segments, stride=span)
        after = []
        for piece in range(pieces):
            product, carried = carry[piece]
            decay = products[piece, rows, :]
            adjoint = local_adjoint[piece, rows, :] + carried
            local_adjoint[piece, rows, :] = adjoint
            products[piece, rows, :] = product
            after.append((product * decay, decay * adjoint))
        return tuple(after)

    ends = lax.fori_loop(
        0,
        span,
        scan_step,
        tuple(
            (
                jnp.ones((segments, piece_width), jnp.float32),
                jnp.zeros((segments, piece_width), jnp.float32),
            )
            for _ in range(pieces)
        ),
        unroll=2,
    )
    product = jnp.concatenate([end[0] for end in ends], axis=1)
    carried = jnp.concatenate([end[1] for end in ends], axis=1)
    whole_product = jnp.ones((1, channels), jnp.float32)
    whole_carry = jnp.zeros((1, channels), jnp.float32)
    for segment in reversed(range(segments)):
        factor = product[segment : segment + 1]
        whole_carry = carried[segment : segment + 1] + factor * whole_carry
        whole_product = whole_product * factor
    totals[me, 0:1, :] = whole_product
    totals[me, 1:2, :] = whole_carry
    pl.semaphore_wait(barrier, count - 1)
    copies = []
    for step in range(1, count):
        copy = pltpu.make_async_remote_copy(
            src_ref=totals.at[me],
            dst_ref=totals.at[me],
            send_sem=send_sem.at[step],
            recv_sem=recv_sem.at[step],
            device_id={"sp": lax.rem(me + step, count)},
            device_id_type=MESH,
        )
        copy.start()
        copies.append(copy)
    for copy in copies:
        copy.wait()

    def join(step, carry_in):
        source = count - 1 - step
        longer = totals[source, 1:2, :] + totals[source, 0:1, :] * carry_in
        return jnp.where(source > me, longer, carry_in)

    carry_in = lax.fori_loop(0, count - 1, join, jnp.zeros((1, channels), jnp.float32))
    entering = [None] * segments
    for segment in reversed(range(segments)):
        entering[segment] = carry_in
        carry_in = carried[segment : segment + 1] + product[segment : segment + 1] * carry_in
    inner = (((1,), (1,)), ((), ()))
    block_span = gate_a.shape[1]
    for block in range(gate_a.shape[0]):
        lower = block * block_span
        upper = lower + block_span
        cols = slice(lower, upper)
        rate = -rate_scale * decay_rate[0:1, cols]
        weight_a = gate_a[block]
        weight_x = gate_x[block]
        for segment in range(segments):
            rows = slice(segment * span, (segment + 1) * span)
            adjoint = local_adjoint[block, rows, :] + products[block, rows, :] * entering[segment][:, cols]
            decay = decay_step[rows, cols]
            keep = keep_gate[rows, cols]
            gate = input_gate[rows, cols]
            conv = conv_x[rows, cols]
            norm = jnp.sqrt(1.0 - decay * decay + floor_square)
            grad_norm = adjoint * conv * gate
            log_grad = adjoint * decay * state_prev[rows, cols] - grad_norm * decay * decay / norm
            keep_adjoint = (log_grad * rate * keep * (1.0 - keep)).astype(jnp.bfloat16)
            input_adjoint = (adjoint * conv * norm * gate * (1.0 - gate)).astype(jnp.bfloat16)
            conv_grad[rows, cols] = (
                adjoint * gate * norm
                + lax.dot_general(keep_adjoint, weight_a, inner, preferred_element_type=jnp.float32)
                + lax.dot_general(
                    input_adjoint, weight_x, inner, preferred_element_type=jnp.float32
                )
            )
    edge = halo.shape[0]
    taps = conv_taps.shape[0]
    back = pltpu.make_async_remote_copy(
        src_ref=conv_grad.at[pl.ds(0, edge)],
        dst_ref=halo,
        send_sem=halo_send,
        recv_sem=halo_recv,
        device_id={"sp": lax.rem(me + count - 1, count)},
        device_id_type=MESH,
    )
    back.start()
    body_rows = tokens - edge
    for segment in range(segments):
        lower = segment * span
        upper = min(lower + span, body_rows)
        result = conv_taps[taps - 1 : taps, :] * conv_grad[lower:upper, :]
        for offset in range(1, taps):
            result = (
                result
                + conv_taps[taps - 1 - offset : taps - offset, :]
                * conv_grad[lower + offset : upper + offset, :]
            )
        grad_x[lower:upper, :] = result
    back.wait()
    conv_grad[tokens : tokens + edge, :] = jnp.where(me == count - 1, 0.0, halo[...])
    result = conv_taps[taps - 1 : taps, :] * conv_grad[body_rows:tokens, :]
    for offset in range(1, taps):
        result = (
            result
            + conv_taps[taps - 1 - offset : taps - offset, :]
            * conv_grad[body_rows + offset : tokens + offset, :]
        )
    grad_x[body_rows:tokens, :] = result


def recurrence(grad_state, decay_step, conv_x, keep_gate, input_gate, state_prev, gate_a, gate_x, decay_rate, conv_taps):
    count = lax.axis_size("sp")
    tokens, channels = grad_state.shape
    blocks = gate_a.shape[0]
    vmem = pl.BlockSpec(memory_space=pltpu.VMEM)
    return pl.pallas_call(
        functools.partial(recurrence_kernel, count),
        out_shape=jax.ShapeDtypeStruct((tokens, channels), jnp.float32),
        in_specs=[vmem] * 10,
        out_specs=vmem,
        scratch_shapes=[
            pltpu.VMEM((blocks, tokens, channels // blocks), jnp.float32),
            pltpu.VMEM((blocks, tokens, channels // blocks), jnp.float32),
            pltpu.VMEM((tokens + 8, channels), jnp.float32),
            pltpu.VMEM((count, 8, channels), jnp.float32),
            pltpu.VMEM((8, channels), jnp.float32),
            pltpu.SemaphoreType.DMA((count,)),
            pltpu.SemaphoreType.DMA((count,)),
            pltpu.SemaphoreType.DMA,
            pltpu.SemaphoreType.DMA,
        ],
        compiler_params=pltpu.CompilerParams(collective_id=1, has_side_effects=True),
        cost_estimate=pl.CostEstimate(
            flops=40 * tokens * channels, bytes_accessed=28 * tokens * channels, transcendentals=tokens * channels
        ),
        name="recurrence",
    )(grad_state, decay_step, conv_x, keep_gate, input_gate, state_prev, gate_a, gate_x, decay_rate[None, :], conv_taps)


def body(
    cotangent,
    routes,
    route_weight,
    expert_rows,
    gate_w,
    up_w,
    down_w,
    in_x,
    in_y,
    state,
    conv_taps,
    gate_a,
    gate_x,
    decay_rate,
    out_weight,
):
    tokens, model_width = cotangent.shape
    experts = lax.axis_size("sp")
    core_count = lax.axis_size("tp")
    core_index = lax.axis_index("tp")
    per_token = routes.shape[1]
    capacity = expert_rows.shape[1] // experts
    half_width = model_width // core_count
    slots = experts * capacity
    chosen = [
        (routes[:, k : k + 1] == jnp.arange(experts, dtype=jnp.int32)[None, :]) for k in range(per_token)
    ]
    named = functools.reduce(jnp.logical_or, chosen).astype(jnp.bfloat16)
    token_range = jnp.arange(tokens, dtype=jnp.int32)
    earlier = (token_range[None, :] < token_range[:, None]).astype(jnp.bfloat16)
    before = jnp.dot(earlier, named, preferred_element_type=jnp.float32).astype(jnp.int32)
    expert_range = jnp.arange(experts, dtype=jnp.int32)[None, :]
    slot_range = jnp.arange(slots, dtype=jnp.int32)
    select = jnp.zeros((slots, tokens), jnp.bool_)
    weighted = jnp.zeros((slots, tokens), jnp.float32)
    picker = jnp.zeros((tokens, slots), jnp.bool_)
    for k in range(per_token):
        place = jnp.sum(jnp.where(chosen[k], before + expert_range * capacity, 0), axis=1)
        hit = slot_range[:, None] == place[None, :]
        select = select | hit
        weighted = weighted + jnp.where(hit, route_weight[:, k][None, :], 0.0)
        picker = picker | (place[:, None] == slot_range[None, :])
    slot_weight = jnp.sum(weighted, axis=1)
    own_cols = lax.dynamic_slice_in_dim(cotangent, core_index * half_width, half_width, 1)
    outgoing = (
        jnp.dot(select.astype(jnp.bfloat16), own_cols, preferred_element_type=jnp.float32)
        * slot_weight[:, None]
    ).astype(jnp.bfloat16)
    arrived = lax.all_to_all(
        outgoing.reshape(experts, capacity, half_width),
        "sp",
        split_axis=0,
        concat_axis=0,
        tiled=True,
    )
    upstream = both_halves(arrived.reshape(-1, half_width))
    saved_rows = expert_rows[0]
    weight_gate = gate_w[0]
    weight_up = up_w[0]
    weight_down = down_w[0]
    pre_gate = jnp.dot(saved_rows, weight_gate, preferred_element_type=jnp.float32)
    pre_up = jnp.dot(saved_rows, weight_up, preferred_element_type=jnp.float32)
    gate_sigmoid = jax.nn.sigmoid(pre_gate)
    silu_value = pre_gate * gate_sigmoid
    active = (silu_value * pre_up).astype(jnp.bfloat16)
    inner = (((1,), (1,)), ((), ()))
    outer = (((0,), (0,)), ((), ()))
    grad_active = lax.dot_general(upstream, weight_down, inner, preferred_element_type=jnp.float32)
    grad_down = lax.dot_general(
        active, upstream, outer, preferred_element_type=jnp.float32
    ).astype(jnp.bfloat16)
    up_adjoint = (grad_active * silu_value).astype(jnp.bfloat16)
    gate_adjoint = (
        grad_active * pre_up * gate_sigmoid * (1.0 + pre_gate * (1.0 - gate_sigmoid))
    ).astype(jnp.bfloat16)
    grad_gate = lax.dot_general(
        saved_rows, gate_adjoint, outer, preferred_element_type=jnp.float32
    ).astype(jnp.bfloat16)
    grad_up = lax.dot_general(
        saved_rows, up_adjoint, outer, preferred_element_type=jnp.float32
    ).astype(jnp.bfloat16)

    def partial_of(core):
        rows_gate = lax.dynamic_slice_in_dim(weight_gate, core * half_width, half_width, 0)
        rows_up = lax.dynamic_slice_in_dim(weight_up, core * half_width, half_width, 0)
        value = lax.dot_general(gate_adjoint, rows_gate, inner, preferred_element_type=jnp.float32)
        value = value + lax.dot_general(
            up_adjoint, rows_up, inner, preferred_element_type=jnp.float32
        )
        return value.astype(jnp.bfloat16)

    arriving = from_other_core(partial_of(core_count - 1 - core_index))
    summed = partial_of(core_index).astype(jnp.float32) + arriving.astype(jnp.float32)
    returning = summed.astype(jnp.bfloat16).reshape(experts, capacity, half_width)
    returned = lax.all_to_all(returning, "sp", split_axis=0, concat_axis=0, tiled=True)
    picked = jnp.dot(
        picker.astype(jnp.bfloat16),
        returned.reshape(slots, half_width),
        preferred_element_type=jnp.float32,
    )
    stream_half = (own_cols.astype(jnp.float32) + picked).astype(jnp.bfloat16)
    stream = both_halves(stream_half)
    y_float = in_y.astype(jnp.float32)
    gelu_y = jax.nn.gelu(y_float, approximate=False)
    gelu_slope = (
        0.5 * (1.0 + lax.erf(y_float * inv_root_two))
        + y_float * jnp.exp(-0.5 * y_float * y_float) * inv_root_tau
    )
    state_float = state.astype(jnp.float32)
    early_y, early_state = lax.optimization_barrier((in_y, state))
    mixed_out = (
        early_state.astype(jnp.float32)
        * jax.nn.gelu(early_y.astype(jnp.float32), approximate=False)
    ).astype(jnp.bfloat16)
    proj_terms = lax.dot_general(
        stream, mixed_out, outer, preferred_element_type=jnp.float32
    ).astype(jnp.bfloat16)
    proj_terms = lax.all_to_all(
        proj_terms.reshape(experts, model_width // experts, -1),
        "sp",
        split_axis=0,
        concat_axis=0,
        tiled=True,
    )
    grad_proj = jnp.sum(proj_terms.astype(jnp.float32), axis=0)
    grad_mixed = jnp.dot(stream, out_weight, preferred_element_type=jnp.float32)
    grad_y = grad_mixed * state_float * gelu_slope
    grad_state = grad_mixed * gelu_y
    tap_count = conv_taps.shape[0]
    channels = in_x.shape[1]
    edge_rows = jnp.concatenate([in_x[tokens - tap_count + 1 :], state[tokens - 1 :]], axis=0)
    prior_rows = shifted(edge_rows, "sp", 1)
    extended = jnp.concatenate([prior_rows[: tap_count - 1], in_x], axis=0).astype(jnp.float32)
    state_prev = jnp.concatenate([prior_rows[tap_count - 1 :], state[:-1]], axis=0).astype(
        jnp.float32
    )
    conv_x = conv_taps[0][None, :] * extended[0:tokens]
    for offset in range(1, tap_count):
        conv_x = conv_x + conv_taps[offset][None, :] * extended[offset : offset + tokens]
    blocks = gate_a.shape[0]
    block_span = gate_a.shape[1]
    conv_b = conv_x.astype(jnp.bfloat16).reshape(tokens, blocks, block_span)
    keep_map = jnp.einsum("tci,cij->tcj", conv_b, gate_a, preferred_element_type=jnp.float32)
    input_map = jnp.einsum("tci,cij->tcj", conv_b, gate_x, preferred_element_type=jnp.float32)
    keep_gate = jax.nn.sigmoid(keep_map).reshape(tokens, channels)
    input_gate = jax.nn.sigmoid(input_map).reshape(tokens, channels)
    decay_step = jnp.exp(-rate_scale * keep_gate * decay_rate[None, :])
    grad_x = recurrence(
        grad_state, decay_step, conv_x, keep_gate, input_gate, state_prev, gate_a, gate_x, decay_rate, conv_taps
    )
    return (grad_gate[None], grad_up[None], grad_down[None], grad_proj, grad_x, grad_y)


def solution(mesh):
    in_specs = (
        P("sp", None),
        P("sp", None),
        P("sp", None),
        P("sp", None, None),
        P("sp", None, "tp"),
        P("sp", None, "tp"),
        P("sp", "tp", None),
        P("sp", "tp"),
        P("sp", "tp"),
        P("sp", "tp"),
        P(None, "tp"),
        P("tp", None, None),
        P("tp", None, None),
        P("tp"),
        P(None, "tp"),
    )
    out_specs = (
        P("sp", None, "tp"),
        P("sp", None, "tp"),
        P("sp", "tp", None),
        P("sp", "tp"),
        P("sp", "tp"),
        P("sp", "tp"),
    )
    return jax.shard_map(body, mesh=mesh, in_specs=in_specs, out_specs=out_specs, check_vma=False)
```

time: 483 us -> 236 us (0.49); the launches traced: 474 us -> 233 us
  local copies, waits for them, and re-layouts: 143 us -> 11.1 us
  blocking collectives: 137 us -> 61 us
  other arithmetic: 40.9 us -> 10.2 us
  Pallas kernels: 0 us -> 26.2 us
  between operations: 15.5 us -> 1.09 us
  matrix products: 64.6 us -> 54.1 us
    all_gather x2 -> x0, blocking collectives: 75.9 us -> none  [carried_in(): pieces = jax.tree.map(lambda part: lax.all_gather(part, axis), value)]
    slice x65 -> x3, local copies, waits for them, and re-layouts: 77.5 us -> 1.65 us  [the longest x1 0.87 us: body(): weighted = weighted + jnp.where(hit, route_weight[:, k][None, :], 0.0)]
    pallas_call x0 -> x1, Pallas kernels: none -> 26.2 us  [recurrence(): pl.pallas_call(functools.partial(recurrence_kernel, count), out_shape=jax...]
    rev x4 -> x0, local copies, waits for them, and re-layouts: 13.9 us -> none  [the longest x1 6.91 us: body(): products = scanned[0][::-1]]
    reduce_scatter x2 -> x0, waiting for transfers between devices: 13 us -> none  [the longest x1 13 us: body(): lax.psum_scatter(partial_value, 'tp', scatter_dimension=1, tiled=True)]
    all_to_all x0 -> x1, starting transfers between devices: none -> 11.2 us  [body(): lax.all_to_all(proj_terms.reshape(experts, model_width // experts, -1), '...]
    mul x16 -> x1, other arithmetic: 10.8 us -> 0.01 us  [body(): expert_range * capacity]
    pad x30 -> x0, local copies, waits for them, and re-layouts: 10.4 us -> none  [body(): lax.associative_scan(linear_combine, (ahead_decay[::-1], grad_state[::-1]...]
  transfers between devices with their start and end apart: 7 -> 6, of which waited for: 3 -> 3; matrix products, arithmetic and copies ran while one was open for 23% -> 21% of each run, Pallas kernels for 0% -> 11%
where the time goes in v1:
time: 236 us; the launch traced here: 233 us
  blocking collectives  61 us (26%)
  matrix products  54.1 us (23%)
  waiting for transfers between devices  49.4 us (21%)
  Pallas kernels  26.2 us (11%)
  starting transfers between devices  20.3 us (9%)
  local copies, waits for them, and re-layouts  11.1 us (5%)
  other arithmetic  10.2 us (4%)
    all_to_all x1, blocking collectives, body(): lax.all_to_all(outgoing.reshape(experts, capacity, half_width), 'sp', spl...  61 us
    all_to_all x1, waiting for transfers between devices, body(): lax.all_to_all(returning, 'sp', split_axis=0, concat_axis=0, tiled=True)  45.8 us
    pallas_call x1, Pallas kernels, recurrence(): pl.pallas_call(functools.partial(recurrence_kernel, count), out_shape=jax...  26.2 us
    all_to_all x1, starting transfers between devices, body(): lax.all_to_all(proj_terms.reshape(experts, model_width // experts, -1), '...  11.2 us
    unnamed x61, local copies, waits for them, and re-layouts  8.05 us
    dot_general x1, matrix products, body(): lax.dot_general(active, upstream, outer, preferred_element_type=jnp.float32)  7.59 us
    dot_general x1, matrix products, body(): lax.dot_general(saved_rows, up_adjoint, outer, preferred_element_type=jnp...  6.42 us
    dot_general x1, matrix products, body(): lax.dot_general(saved_rows, gate_adjoint, outer, preferred_element_type=j...  5.46 us
  transfers between devices with their start and end apart: 6, of which 3 were waited for; matrix products, arithmetic and copies ran while one was open for 21% of the time, Pallas kernels for 11%

profile of v1, /device:TPU:4, one launch (start us, length us, event | category | flops | bytes accessed | tf_op | source)
XLA Modules:
  0.0 233.4 jit_solution(16415382189818263935)
XLA Ops:
  3.0 2.5 %fusion.8 = bf16[1152,1024]{1,0:T(8,128)(2,1)S(1)} fusion(f32[1152]{0:T(1024)S(1)} %add_reduce_fusion, s32[384]{0:T(512)S(1)} %get-tuple-element.23, s32[384]{0:T(512)S(1)} %get-tuple-element.22, bf16[384,2048]{1,0:T(8,128)(2,1)} %param.15, s32[]{:T(128)S(6)} %select_n.50), kind=kOutput, calls=%fused_computation.14 | convolution fusion | flops 909656064 | bytes 3153412 | tf_op jit(solution)/shard_map/dot_general | solution.py:276
  5.5 61.0 %all_to_all.15 = bf16[16,72,1024]{2,1,0:T(8,128)(2,1)} all-to-all(bf16[16,72,1024]{2,1,0:T(8,128)(2,1)S(1)} %bitcast.88), channel_id=1, replica_groups=mesh['sp'=16,'tp'=2] {'sp'}, dimensions={0} | all-to-all | bytes 4718592 | tf_op jit(solution)/shard_map/all_to_all | solution.py:279
  66.5 4.6 %fusion.4 = f32[1152,512]{1,0:T(8,128)S(1)} fusion(bf16[1,1152,2048]{2,1,0:T(8,128)(2,1)} %param.18, bf16[1,2048,512]{2,1,0:T(8,128)(2,1)S(1)} %copy-done), kind=kOutput, calls=%fused_computation.8 | convolution fusion | flops 2415919104 | bytes 9175040 | tf_op jit(solution)/shard_map/dot_general | solution.py:291
  71.1 5.3 %fusion.6 = f32[1152,512]{1,0:T(8,128)S(1)} fusion(bf16[1,1152,2048]{2,1,0:T(8,128)(2,1)} %param.18, bf16[1,2048,512]{2,1,0:T(8,128)(2,1)S(1)} %copy-done.11), kind=kOutput, calls=%fused_computation.10 | convolution fusion | flops 2415919104 | bytes 9175040 | tf_op jit(solution)/shard_map/dot_general | solution.py:292
  76.5 3.6 %broadcast_select_fusion.1 = (bf16[1152,1024]{1,0:T(8,128)(2,1)S(1)}, bf16[1152,1024]{1,0:T(8,128)(2,1)S(1)}) fusion(bf16[1152,1024]{1,0:T(8,128)(2,1)} %collective-permute-done, pred[]{:T(512)S(6)} %eq.42, bf16[16,72,1024]{2,1,0:T(8,128)(2,1)} %all_to_all.15), kind=kLoop, calls=%fused_computation.32 | loop fusion | flops 2359296 | bytes 9437185 | tf_op jit(solution)/shard_map/jit(_where)/select_n | solution.py:33
  80.3 3.5 %multiply_convert_fusion.1 = (bf16[1152,512]{1,0:T(8,128)(2,1)S(1)}, bf16[1152,512]{1,0:T(8,128)(2,1)S(1)}) fusion(f32[1152,512]{1,0:T(8,128)S(1)} %fusion.4, f32[1152,512]{1,0:T(8,128)S(1)} %fusion.6, bf16[1,512,2048]{2,1,0:T(8,128)(2,1)S(1)} %copy-done.23, bf16[1152,1024]{1,0:T(8,128)(2,1)S(1)} %get-tuple-element.33, ...), kind=kOutput, calls=%fused_computation.27 | convolution fusion | flops 2433024000 | bytes 13893632 | tf_op jit(solution)/shard_map/dot_general | solution.py:298
  83.9 1.4 fusion.46
  85.4 1.5 fusion.10
  88.9 2.7 %collective-permute-done.1 = bf16[1152,1024]{1,0:T(8,128)(2,1)S(1)} collective-permute-done((bf16[1152,1024]{1,0:T(8,128)(2,1)S(1)}, bf16[1152,1024]{1,0:T(8,128)(2,1)S(1)}, u32[]{:S(2)}, u32[]{:S(2)}) %collective-permute-start.1) | collective-permute-done | bytes 2359328 | tf_op jit(solution)/shard_map/ppermute | solution.py:26
  91.6 2.9 %add_convert_fusion = bf16[1152,1024]{1,0:T(8,128)(2,1)} fusion(bf16[1152,1024]{1,0:T(8,128)(2,1)S(1)} %collective-permute-done.1, f32[1152,1024]{1,0:T(8,128)S(1)} %fusion.49, bf16[1152,512]{1,0:T(8,128)(2,1)S(1)} %get-tuple-element.30, bf16[1,2048,512]{2,1,0:T(8,128)(2,1)S(1)} %copy-done.11, s32[]{:T(128)S(6)} %select_n.50), kind=kOutput, calls=%fused_computation.12 | convolution fusion | flops 1215037440 | bytes 11665412 | tf_op jit(solution)/shard_map/dot_general | solution.py:317
  94.5 4.9 %all-to-all-start.1 = ((bf16[16,72,1024]{2,1,0:T(8,128)(2,1)}), bf16[16,72,1024]{2,1,0:T(8,128)(2,1)S(1)}, u32[]{:S(2)}, u32[]{:S(2)}) async-start(bf16[16,72,1024]{2,1,0:T(8,128)(2,1)} %bitcast.15), calls=%async_computation.1 | async-start | bytes 4718592 | tf_op jit(solution)/shard_map/all_to_all | solution.py:325
  99.5 3.6 %collective-permute-start.3 = (bf16[4,512]{1,0:T(4,128)(2,1)S(1)}, bf16[4,512]{1,0:T(4,128)(2,1)S(1)}, u32[]{:S(2)}, u32[]{:S(2)}) collective-permute-start(bf16[4,512]{1,0:T(4,128)(2,1)S(1)} %pad_maximum_fusion.10), channel_id=1, source_target_pairs={{0,2},{2,4},{4,6},{6,8},{8,10},{10,12},{12,14},{14,16},{16,18},{18... | collective-permute-start | bytes 12296 | tf_op jit(solution)/shard_map/ppermute | solution.py:22
  103.1 45.8 %all-to-all-done.1 = bf16[16,72,1024]{2,1,0:T(8,128)(2,1)S(1)} async-done(((bf16[16,72,1024]{2,1,0:T(8,128)(2,1)}), bf16[16,72,1024]{2,1,0:T(8,128)(2,1)S(1)}, u32[]{:S(2)}, u32[]{:S(2)}) %all-to-all-start.1) | async-done | bytes 2359328 | tf_op jit(solution)/shard_map/all_to_all | solution.py:325
  148.9 2.4 %add_convert_fusion.1 = bf16[384,1024]{1,0:T(8,128)(2,1)S(1)} fusion(bf16[1152,1024]{1,0:T(8,128)(2,1)S(1)} %bitcast.87, s32[384]{0:T(512)S(1)} %get-tuple-element.23, s32[384]{0:T(512)S(1)} %get-tuple-element.22, bf16[384,2048]{1,0:T(8,128)(2,1)} %param.15, s32[]{:T(128)S(6)} %select_n.50), kind=kOutput, calls=%fused_computation.51 | convolution fusion | flops 908476416 | bytes 3935236 | tf_op jit(solution)/shard_map/dot_general | solution.py:326
  153.8 4.1 %convolution_convert_fusion = bf16[2048,512]{1,0:T(8,128)(2,1)} fusion(bf16[384,1024]{1,0:T(8,128)(2,1)S(1)} %get-tuple-element.35, bf16[384,1024]{1,0:T(8,128)(2,1)S(1)} %get-tuple-element.34, bf16[384,512]{1,0:T(8,128)(2,1)S(1)} %copy-done.25, bf16[384,512]{1,0:T(8,128)(2,1)S(1)} %copy-done.17), kind=kOutput, calls=%fused_computation.22 | convolution fusion | flops 822870016 | bytes 4456448 | tf_op jit(solution)/shard_map/dot_general | solution.py:345
  157.9 11.2 %all-to-all-start.2 = ((bf16[16,128,512]{2,1,0:T(8,128)(2,1)}), bf16[16,128,512]{2,1,0:T(8,128)(2,1)}, u32[]{:S(2)}, u32[]{:S(2)}) async-start(bf16[16,128,512]{2,1,0:T(8,128)(2,1)} %bitcast.17), calls=%async_computation.2 | async-start | bytes 4194304 | tf_op jit(solution)/shard_map/all_to_all | solution.py:348
  173.6 5.5 %fusion.23 = bf16[1,2048,512]{1,2,0:T(8,128)(2,1)S(1)} fusion(bf16[1152,512]{1,0:T(8,128)(2,1)S(1)} %copy-done.4, bf16[1,1152,2048]{2,1,0:T(8,128)(2,1)} %param.18), kind=kOutput, calls=%fused_computation.24 | convolution fusion | flops 2416967680 | bytes 7995392 | tf_op jit(solution)/shard_map/dot_general | solution.py:306
  179.1 2.5 %copy.35 = bf16[1,2048,512]{2,1,0:T(8,128)(2,1)} copy(bf16[1,2048,512]{1,2,0:T(8,128)(2,1)S(1)} %fusion.23) | data formatting | bytes 4194304
  181.6 6.4 %fusion.20 = bf16[1,2048,512]{1,2,0:T(8,128)(2,1)} fusion(bf16[1152,512]{1,0:T(8,128)(2,1)S(1)} %copy-done.6, bf16[1,1152,2048]{2,1,0:T(8,128)(2,1)} %param.18), kind=kOutput, calls=%fused_computation.23 | convolution fusion | flops 2416967680 | bytes 7995392 | tf_op jit(solution)/shard_map/dot_general | solution.py:309
  188.0 4.1 %copy.36 = bf16[1,2048,512]{2,1,0:T(8,128)(2,1)} copy(bf16[1,2048,512]{1,2,0:T(8,128)(2,1)} %fusion.20) | data formatting | bytes 4194304
  192.1 7.6 %fusion.26 = bf16[1,512,2048]{2,1,0:T(8,128)(2,1)} fusion(bf16[1152,1024]{1,0:T(8,128)(2,1)} %copy-done.10, bf16[1152,1024]{1,0:T(8,128)(2,1)S(1)} %copy-done.9, f32[1152,512]{1,0:T(8,128)} %copy-done.28, f32[1152,512]{1,0:T(8,128)} %copy-done.27), kind=kOutput, calls=%fused_computation.25 | convolution fusion | flops 2429943808 | bytes 11534336 | tf_op jit(solution)/shard_map/dot_general | solution.py:299
  199.8 3.8 %fusion.127 = (f32[384,512]{1,0:T(8,128)}, f32[384,512]{1,0:T(8,128)}) fusion(bf16[384,512]{1,0:T(8,128)(2,1)S(1)} %copy-done.26, bf16[384,512]{1,0:T(8,128)(2,1)S(1)} %copy-done.18, bf16[2048,512]{1,0:T(8,128)(2,1)S(1)} %copy-done.24, bf16[384,1024]{1,0:T(8,128)(2,1)S(1)} %copy-done.15, bf16[384,1024]{1,0:T(8,128)(2,1)S(1)} %copy-done.13), kind=kOutput, calls=%fused_computation.148 | convolution fusion | flops 823590912 | bytes 6029312 | tf_op jit(solution)/shard_map/dot_general | solution.py:356
  203.6 26.2 %recurrence.1 = f32[384,512]{1,0:T(8,128)} custom-call(f32[384,512]{1,0:T(8,128)} %get-tuple-element.37.grad_state, f32[384,512]{1,0:T(8,128)} %multiply_exponential_fusion.decay_step, f32[384,512]{1,0:T(8,128)} %get-tuple-element.29.conv_x, f32[384,512]{1,0:T(8,128)} %copy-done.2, f32[384,512]{1,0:T(8,128)} %copy.40.input_gate, ...), custom_call_target="tpu_custom_call" | custom-call | flops 7864320 | bytes 5505024 | tf_op jit(solution)/shard_map/recurrence/pallas_call | solution.py:206
  229.8 2.7 %convert_reduce_fusion = f32[128,512]{1,0:T(8,128)} fusion(bf16[16,128,512]{2,1,0:T(8,128)(2,1)} %all-to-all-done.2), kind=kLoop, calls=%fused_computation.13 | loop fusion | flops 2031616 | bytes 2359296 | tf_op jit(solution)/shard_map/reduce_sum | solution.py:355
  (87 shorter events, 12.4 us)
Async XLA Ops:
  0.6 65.9 %copy-start = (bf16[1,2048,512]{2,1,0:T(8,128)(2,1)S(1)}, bf16[1,2048,512]{2,1,0:T(8,128)(2,1)}, u32[]{:S(2)}) copy-start(bf16[1,2048,512]{2,1,0:T(8,128)(2,1)} %param.19) | copy-start | bytes 6291460
  66.5 10.0 %collective-permute-start = (bf16[1152,1024]{1,0:T(8,128)(2,1)}, bf16[1152,1024]{1,0:T(8,128)(2,1)}, u32[]{:S(2)}, u32[]{:S(2)}) collective-permute-start(bf16[1152,1024]{1,0:T(8,128)(2,1)} %bitcast.1), channel_id=1, source_target_pairs={{0,1},{1,0},{2,3},{3,2},{4,5},{5,4},{6,7},{7,6},{8,9},{9,8},{10,11... | collective-permute-start | bytes 7077896 | tf_op jit(solution)/shard_map/ppermute | solution.py:26
  66.5 4.6 %copy-start.11 = (bf16[1,2048,512]{2,1,0:T(8,128)(2,1)S(1)}, bf16[1,2048,512]{2,1,0:T(8,128)(2,1)}, u32[]{:S(2)}) copy-start(bf16[1,2048,512]{2,1,0:T(8,128)(2,1)} %param.20) | copy-start | bytes 6291460
  71.1 9.0 %copy-start.27 = (f32[1152,512]{1,0:T(8,128)}, f32[1152,512]{1,0:T(8,128)S(1)}, u32[]{:S(2)}) copy-start(f32[1152,512]{1,0:T(8,128)S(1)} %fusion.4) | copy-start | bytes 7077892
  76.5 3.9 %copy-start.23 = (bf16[1,512,2048]{2,1,0:T(8,128)(2,1)S(1)}, bf16[1,512,2048]{2,1,0:T(8,128)(2,1)}, u32[]{:S(2)}) copy-start(bf16[1,512,2048]{2,1,0:T(8,128)(2,1)} %param.21) | copy-start | bytes 6291460
  80.1 3.8 %copy-start.8 = (bf16[1152,1024]{1,0:T(8,128)(2,1)}, bf16[1152,1024]{1,0:T(8,128)(2,1)S(1)}, u32[]{:S(2)}) copy-start(bf16[1152,1024]{1,0:T(8,128)(2,1)S(1)} %get-tuple-element.32) | copy-start | bytes 7077892
  83.9 7.7 %copy-start.5 = (bf16[1152,512]{1,0:T(8,128)(2,1)}, bf16[1152,512]{1,0:T(8,128)(2,1)S(1)}, u32[]{:S(2)}) copy-start(bf16[1152,512]{1,0:T(8,128)(2,1)S(1)} %get-tuple-element.30) | copy-start | bytes 3538948
  86.9 4.7 %collective-permute-start.1 = (bf16[1152,1024]{1,0:T(8,128)(2,1)S(1)}, bf16[1152,1024]{1,0:T(8,128)(2,1)S(1)}, u32[]{:S(2)}, u32[]{:S(2)}) collective-permute-start(bf16[1152,1024]{1,0:T(8,128)(2,1)S(1)} %fusion.10), channel_id=1, source_target_pairs={{0,1},{1,0},{2,3},{3,2},{4,5},{5,4},{6,7},{7,6},{8,9},{9,8},{10,11... | collective-permute-start | bytes 7077896 | tf_op jit(solution)/shard_map/ppermute | solution.py:26
  94.5 4.9 %copy-start.17 = (bf16[384,512]{1,0:T(8,128)(2,1)S(1)}, bf16[384,512]{1,0:T(8,128)(2,1)}, u32[]{:S(2)}) copy-start(bf16[384,512]{1,0:T(8,128)(2,1)} %param.24) | copy-start | bytes 1179652
  94.5 5.0 %copy-start.16 = (bf16[384,512]{1,0:T(8,128)(2,1)S(1)}, bf16[384,512]{1,0:T(8,128)(2,1)}, u32[]{:S(2)}) copy-start(bf16[384,512]{1,0:T(8,128)(2,1)} %param.22) | copy-start | bytes 1179652
  94.5 54.4 %all-to-all-start.1 = ((bf16[16,72,1024]{2,1,0:T(8,128)(2,1)}), bf16[16,72,1024]{2,1,0:T(8,128)(2,1)S(1)}, u32[]{:S(2)}, u32[]{:S(2)}) async-start(bf16[16,72,1024]{2,1,0:T(8,128)(2,1)} %bitcast.15), calls=%async_computation.1 | async-start | bytes 4718592 | tf_op jit(solution)/shard_map/all_to_all | solution.py:325
  99.5 51.9 %collective-permute-start.3 = (bf16[4,512]{1,0:T(4,128)(2,1)S(1)}, bf16[4,512]{1,0:T(4,128)(2,1)S(1)}, u32[]{:S(2)}, u32[]{:S(2)}) collective-permute-start(bf16[4,512]{1,0:T(4,128)(2,1)S(1)} %pad_maximum_fusion.10), channel_id=1, source_target_pairs={{0,2},{2,4},{4,6},{6,8},{8,10},{10,12},{12,14},{14,16},{16,18},{18... | collective-permute-start | bytes 12296 | tf_op jit(solution)/shard_map/ppermute | solution.py:22
  151.3 2.4 %collective-permute-start.2 = (bf16[384,1024]{1,0:T(8,128)(2,1)S(1)}, bf16[384,1024]{1,0:T(8,128)(2,1)S(1)}, u32[]{:S(2)}, u32[]{:S(2)}) collective-permute-start(bf16[384,1024]{1,0:T(8,128)(2,1)S(1)} %add_convert_fusion.1), channel_id=1, source_target_pairs={{0,1},{1,0},{2,3},{3,2},{4,5},{5,4},{6,7},{7,6},{8,9},{9,8},{10,11... | collective-permute-start | bytes 2359304 | tf_op jit(solution)/shard_map/ppermute | solution.py:26
  153.8 4.1 %copy-start.12 = (bf16[384,1024]{1,0:T(8,128)(2,1)}, bf16[384,1024]{1,0:T(8,128)(2,1)S(1)}, u32[]{:S(2)}) copy-start(bf16[384,1024]{1,0:T(8,128)(2,1)S(1)} %get-tuple-element.34) | copy-start | bytes 2359300
  153.8 4.1 %copy-start.14 = (bf16[384,1024]{1,0:T(8,128)(2,1)}, bf16[384,1024]{1,0:T(8,128)(2,1)S(1)}, u32[]{:S(2)}) copy-start(bf16[384,1024]{1,0:T(8,128)(2,1)S(1)} %get-tuple-element.35) | copy-start | bytes 2359300
  157.9 11.2 %copy-start.19 = (bf16[4,128,128]{2,1,0:T(8,128)(2,1)S(1)}, bf16[4,128,128]{2,1,0:T(8,128)(2,1)}, u32[]{:S(2)}) copy-start(bf16[4,128,128]{2,1,0:T(8,128)(2,1)} %gate_a.1) | copy-start | bytes 393220
  157.9 71.8 %all-to-all-start.2 = ((bf16[16,128,512]{2,1,0:T(8,128)(2,1)}), bf16[16,128,512]{2,1,0:T(8,128)(2,1)}, u32[]{:S(2)}, u32[]{:S(2)}) async-start(bf16[16,128,512]{2,1,0:T(8,128)(2,1)} %bitcast.17), calls=%async_computation.2 | async-start | bytes 4194304 | tf_op jit(solution)/shard_map/all_to_all | solution.py:348
  188.0 4.1 %copy-start.9 = (bf16[1152,1024]{1,0:T(8,128)(2,1)S(1)}, bf16[1152,1024]{1,0:T(8,128)(2,1)}, u32[]{:S(2)}) copy-start(bf16[1152,1024]{1,0:T(8,128)(2,1)} %copy-done.8) | copy-start | bytes 7077892
  192.1 7.6 %copy-start.13 = (bf16[384,1024]{1,0:T(8,128)(2,1)S(1)}, bf16[384,1024]{1,0:T(8,128)(2,1)}, u32[]{:S(2)}) copy-start(bf16[384,1024]{1,0:T(8,128)(2,1)} %copy-done.12) | copy-start | bytes 2359300
  192.1 7.6 %copy-start.15 = (bf16[384,1024]{1,0:T(8,128)(2,1)S(1)}, bf16[384,1024]{1,0:T(8,128)(2,1)}, u32[]{:S(2)}) copy-start(bf16[384,1024]{1,0:T(8,128)(2,1)} %copy-done.14) | copy-start | bytes 2359300
  192.1 7.6 %copy-start.18 = (bf16[384,512]{1,0:T(8,128)(2,1)S(1)}, bf16[384,512]{1,0:T(8,128)(2,1)}, u32[]{:S(2)}) copy-start(bf16[384,512]{1,0:T(8,128)(2,1)} %param.24) | copy-start | bytes 1179652
  192.1 7.6 %copy-start.24 = (bf16[2048,512]{1,0:T(8,128)(2,1)S(1)}, bf16[2048,512]{1,0:T(8,128)(2,1)}, u32[]{:S(2)}) copy-start(bf16[2048,512]{1,0:T(8,128)(2,1)} %param.29) | copy-start | bytes 6291460
  192.1 7.6 %copy-start.26 = (bf16[384,512]{1,0:T(8,128)(2,1)S(1)}, bf16[384,512]{1,0:T(8,128)(2,1)}, u32[]{:S(2)}) copy-start(bf16[384,512]{1,0:T(8,128)(2,1)} %param.23) | copy-start | bytes 1179652
  203.6 29.7 %copy-start.1 = (bf16[1,2048,512]{2,1,0:T(8,128)(2,1)S(1)}, bf16[1,2048,512]{2,1,0:T(8,128)(2,1)}, u32[]{:S(2)}) copy-start(bf16[1,2048,512]{2,1,0:T(8,128)(2,1)} %param.19) | copy-start | bytes 6291460
  (11 other events, 28.9 us)
